TPU v7x, 32 devices: a whole 2x2x4 slice. The times are simulated.
32 devices in a mesh: sp: 8 (over z, y), tp: 4 (over x, core).
Axes of the slice: x: 2, y: 2, z: 4, core: 2. Of those that a mesh axis runs over, the one named last changes fastest.
Arguments:
- queries: bfloat16 [4096, 2048], P('sp', 'tp'), may hold values from -6 to 6
- keys: bfloat16 [4096, 512], P('sp', 'tp'), may hold values from -6 to 6
- values: bfloat16 [4096, 512], P('sp', 'tp'), may hold values from -6 to 6
- residual: bfloat16 [4096, 2048], P(('sp', 'tp')), may hold values from -0.119628906 to 0.119628906
- out_proj: bfloat16 [2048, 2048], replicated, may hold values from -0.125 to 0.125
- query_gain: float32 [128], replicated, may hold values from 0.7 to 7
- key_gain: float32 [128], replicated, may hold values from 0.7 to 7
- norm_gain: float32 [2048], replicated, may hold values from 0.1 to 1.9
- routes: int32 [4096, 4], P(('sp', 'tp')), may hold values from 0 to 31, all different within a row; in each aligned block of 128 rows (0 to 127, 128 to 255, ...) at most 32 rows name the same one
- route_weight: float32 [4096, 4], P(('sp', 'tp')), may hold values from 0.1 to 1
- expert_gate: bfloat16 [32, 2048, 256], P(('sp', 'tp')), may hold values from -0.125 to 0.125
- expert_up: bfloat16 [32, 2048, 256], P(('sp', 'tp')), may hold values from -0.125 to 0.125
- expert_down: bfloat16 [32, 256, 2048], P(('sp', 'tp')), may hold values from -0.375 to 0.375
- shared_gate: bfloat16 [2048, 256], replicated, may hold values from -0.125 to 0.125
- shared_up: bfloat16 [2048, 256], replicated, may hold values from -0.125 to 0.125
- shared_down: bfloat16 [256, 2048], replicated, may hold values from -0.375 to 0.375
Outputs:
- layer_out: bfloat16 [4096, 2048], P(('sp', 'tp'))
Inputs may be any that keep to these rules, and one draw needn't show every extreme that they name: In the rows of one device (aligned blocks of 128 tokens), no expert is named by more than 32 routes; some expert is named by exactly 32 routes of some device; the 4 experts of a token differ.
All inputs are finite; a program needn't handle non-finite values.
Results may differ from a plain program's by a relative error of at most 0.023.
The roundings to bfloat16 on the way count: a program that leaves them out, or rounds other values in their place, can miss the bound.
Values may be sent and summed in bfloat16 or wider, within the bound.
A program may use at most 128 MiB of HBM per device.

v0:
```python
import math
import jax
import jax.numpy as jnp
from jax import lax
from jax.sharding import PartitionSpec as P

HEADS = 16
KV_HEADS = 4
GRID_W = 64
EPS = 1e-06
THETA = 10000.0


def rotate_pairs(block, cosine, sine):
    first, second = jnp.split(block, 2, axis=-1)
    return jnp.concatenate(
        [first * cosine - second * sine, second * cosine + first * sine], axis=-1
    )


def normed_rotary(source, gain, heads, offset):
    count = source.shape[0]
    width = gain.shape[0]
    values_f = source.astype(jnp.float32).reshape(count, heads, width)
    values_f = (
        values_f * lax.rsqrt(jnp.mean(values_f * values_f, axis=-1, keepdims=True) + EPS) * gain
    )
    position = offset + jnp.arange(count, dtype=jnp.int32)
    grid_row = (position // GRID_W).astype(jnp.float32)
    grid_col = (position % GRID_W).astype(jnp.float32)
    quarter = width // 4
    inverse = jnp.power(THETA, -4.0 * jnp.arange(quarter, dtype=jnp.float32) / width)
    row_angle = (grid_row[:, None] * inverse[None, :])[:, None, :]
    col_angle = (grid_col[:, None] * inverse[None, :])[:, None, :]
    row_half, col_half = jnp.split(values_f, 2, axis=-1)
    turned = jnp.concatenate(
        [
            rotate_pairs(row_half, jnp.cos(row_angle), jnp.sin(row_angle)),
            rotate_pairs(col_half, jnp.cos(col_angle), jnp.sin(col_angle)),
        ],
        axis=-1,
    )
    return turned.reshape(count, heads * width).astype(jnp.bfloat16)


def expert_apply(arrived, expert_gate, expert_up, expert_down):
    sources, slots, width = arrived.shape
    local = expert_gate.shape[0]
    grouped = arrived.reshape(sources // local, local, slots, width)
    gate_part = jnp.einsum(
        "sech,ehf->secf", grouped, expert_gate, preferred_element_type=jnp.float32
    )
    up_part = jnp.einsum("sech,ehf->secf", grouped, expert_up, preferred_element_type=jnp.float32)
    hidden_e = (jax.nn.silu(gate_part) * up_part).astype(jnp.bfloat16)
    result = jnp.einsum("secf,efh->sech", hidden_e, expert_down, preferred_element_type=jnp.float32)
    return result.astype(jnp.bfloat16).reshape(sources, slots, width)


def body(
    queries,
    keys,
    values,
    residual,
    out_proj,
    query_gain,
    key_gain,
    norm_gain,
    routes,
    route_weight,
    expert_gate,
    expert_up,
    expert_down,
    shared_gate,
    shared_up,
    shared_down,
):
    tok_local = queries.shape[0]
    width = query_gain.shape[0]
    group = HEADS // KV_HEADS
    kv_local = keys.shape[1] // width
    scale = 1.0 / math.sqrt(width)
    offset = lax.axis_index("sp") * tok_local
    q_rot = normed_rotary(queries, query_gain, kv_local * group, offset)
    k_rot = normed_rotary(keys, key_gain, kv_local, offset)
    query_3d = q_rot.reshape(tok_local, kv_local, group, width).transpose(1, 2, 0, 3)
    query_3d = query_3d.reshape(kv_local, group * tok_local, width)
    start_state = (
        jnp.full((kv_local, group * tok_local), -jnp.inf, jnp.float32),
        jnp.zeros((kv_local, group * tok_local), jnp.float32),
        jnp.zeros((kv_local, group * tok_local, width), jnp.float32),
    )
    key_piece = lax.all_gather(k_rot, "sp", axis=0, tiled=True)
    value_piece = lax.all_gather(values, "sp", axis=0, tiled=True)
    count = key_piece.shape[0]
    block = math.gcd(count, 512)

    def one_block(index_block, state):
        running_max, running_sum, accum = state
        key_rows = lax.dynamic_slice_in_dim(key_piece, index_block * block, block, 0)
        value_rows = lax.dynamic_slice_in_dim(value_piece, index_block * block, block, 0)
        key_3d = key_rows.reshape(block, kv_local, width)
        value_3d = value_rows.reshape(block, kv_local, width)
        scores = (
            jnp.einsum("gqd,kgd->gqk", query_3d, key_3d, preferred_element_type=jnp.float32) * scale
        )
        new_max = jnp.maximum(running_max, jnp.max(scores, axis=-1))
        weights = jnp.exp(scores - new_max[..., None])
        factor = jnp.exp(running_max - new_max)
        new_sum = running_sum * factor + jnp.sum(weights, axis=-1)
        added = jnp.einsum(
            "gqk,kgd->gqd",
            weights.astype(jnp.bfloat16),
            value_3d,
            preferred_element_type=jnp.float32,
        )
        return (new_max, new_sum, accum * factor[..., None] + added)

    final_max, final_sum, final_acc = lax.fori_loop(0, count // block, one_block, start_state)
    attn_local = (final_acc / final_sum[..., None]).astype(jnp.bfloat16)
    attn_local = attn_local.reshape(kv_local, group, tok_local, width).transpose(2, 0, 1, 3)
    attn_local = attn_local.reshape(tok_local, kv_local * group * width)
    all_heads = lax.all_to_all(attn_local, "tp", split_axis=0, concat_axis=1, tiled=True)
    projected = jnp.dot(all_heads, out_proj, preferred_element_type=jnp.float32)
    hidden1 = (residual.astype(jnp.float32) + projected).astype(jnp.bfloat16)
    hidden_f = hidden1.astype(jnp.float32)
    normed = (
        hidden_f
        * lax.rsqrt(jnp.mean(hidden_f * hidden_f, axis=-1, keepdims=True) + EPS)
        * norm_gain
    ).astype(jnp.bfloat16)
    rows_local = normed.shape[0]
    top_count = routes.shape[1]
    pair_count = rows_local * top_count
    expert_total = expert_gate.shape[0] * lax.axis_size("sp") * lax.axis_size("tp")
    capacity = max(2, 2 * rows_local * top_count // expert_total)
    flat_routes = routes.reshape(pair_count)
    one_hot = (flat_routes[:, None] == jnp.arange(expert_total, dtype=jnp.int32)[None, :]).astype(
        jnp.float32
    )
    lower = (jnp.arange(pair_count)[:, None] >= jnp.arange(pair_count)[None, :]).astype(jnp.float32)
    running_count = jnp.dot(lower, one_hot, precision=lax.Precision.HIGHEST)
    slot_place = (jnp.sum(running_count * one_hot, axis=1) - 1.0).astype(jnp.int32)
    slot_index = flat_routes * capacity + slot_place
    slot_total = expert_total * capacity
    placement = (jnp.arange(slot_total, dtype=jnp.int32)[:, None] == slot_index[None, :]).astype(
        jnp.bfloat16
    )
    placement = jnp.sum(placement.reshape(slot_total, rows_local, top_count), axis=2)
    send_rows = jnp.dot(placement, normed, preferred_element_type=jnp.float32).astype(jnp.bfloat16)
    send_rows = send_rows.reshape(expert_total, capacity, normed.shape[1])
    shared_hidden = (
        jax.nn.silu(jnp.dot(normed, shared_gate, preferred_element_type=jnp.float32))
        * jnp.dot(normed, shared_up, preferred_element_type=jnp.float32)
    ).astype(jnp.bfloat16)
    shared_out = jnp.dot(shared_hidden, shared_down, preferred_element_type=jnp.float32)
    processed = expert_apply(
        lax.all_to_all(send_rows, ("sp", "tp"), split_axis=0, concat_axis=0, tiled=True),
        expert_gate,
        expert_up,
        expert_down,
    )
    returned = lax.all_to_all(processed, ("sp", "tp"), split_axis=0, concat_axis=0, tiled=True)
    returned = returned.reshape(slot_total, normed.shape[1])
    routed = (
        returned[slot_index].reshape(rows_local, top_count, normed.shape[1]).astype(jnp.float32)
    )
    mixed = jnp.einsum("tk,tkd->td", route_weight, routed) + shared_out
    return (hidden_f + mixed).astype(jnp.bfloat16)


def solution(mesh):
    placed = (
        P("sp", "tp"),
        P("sp", "tp"),
        P("sp", "tp"),
        P(("sp", "tp"), None),
        P(),
        P(),
        P(),
        P(),
        P(("sp", "tp"), None),
        P(("sp", "tp"), None),
        P(("sp", "tp"), None, None),
        P(("sp", "tp"), None, None),
        P(("sp", "tp"), None, None),
        P(),
        P(),
        P(),
    )
    return jax.shard_map(
        body, mesh=mesh, in_specs=placed, out_specs=P(("sp", "tp"), None), check_vma=False
    )
```

profile of v0, /device:TPU:0, one launch (start us, length us, event | category | flops | bytes accessed | tf_op | source)
XLA Modules:
  0.0 420.8 jit_solution(3090994777994951920)
XLA Ops:
  6.6 1.1 copy.35
  7.7 0.7 fusion.43
  8.5 0.6 fusion.62
  9.0 0.7 pad_maximum_fusion
  9.8 0.7 all-gather.4.cloned.1.call-update
  10.5 1.4 reshape.480
  11.9 0.6 multiply_reduce_fusion.2
  12.6 1.9 multiply_cosine_fusion.1
  14.5 0.7 multiply_multiply_fusion
  15.2 1.8 fusion.37
  17.0 1.6 maximum_bitcast_fusion
  19.2 32.9 %all-gather.6.cloned.1.call-done = bf16[4096,1,128]{0,2,1:T(8,128)(2,1)} async-done(((bf16[512,1,128]{0,2,1:T(8,128)(2,1)}), bf16[4096,1,128]{0,2,1:T(8,128)(2,1)}) %all-gather.6.cloned.1.call-update) | async-done | bytes 1048592 | tf_op jit(solution)/shard_map/all_gather | solution.py:92
  52.1 41.4 %all-gather.4.cloned.1.call-done = bf16[4096,128]{1,0:T(8,128)(2,1)} async-done(((bf16[512,128]{1,0:T(8,128)(2,1)}), bf16[4096,128]{1,0:T(8,128)(2,1)}) %all-gather.4.cloned.1.call-update) | async-done | bytes 1048592 | tf_op jit(solution)/shard_map/all_gather | solution.py:93
  93.6 73.7 %while.18 = (s32[]{:T(128)}, f32[1,2048]{1,0:T(1,128)S(1)}, f32[1,2048]{1,0:T(1,128)S(1)}, f32[1,2048,128]{2,1,0:T(8,128)S(1)}, bf16[4096,128]{0,1:T(8,128)(2,1)...) while((s32[]{:T(128)}, f32[1,2048]{1,0:T(1,128)S(1)}, ...), condition=%wide.region_5.6_spmd.clone, body=%wide.region_2.5_spmd.clone.sunk | while | flops 546056192 | bytes 32374984 | solution.py:118
  93.6 3.6 multiply_reduce_fusion.4
  97.2 3.0 fusion.96
  100.3 0.3 copy-done.1
  100.6 2.1 fusion.98
  102.8 3.6 multiply_reduce_fusion.4
  106.4 3.0 fusion.96
  109.5 0.3 copy-done.1
  109.8 2.1 fusion.98
  112.0 3.6 multiply_reduce_fusion.4
  115.6 3.0 fusion.96
  118.7 0.3 copy-done.1
  119.0 2.1 fusion.98
  121.2 3.6 multiply_reduce_fusion.4
  124.8 3.0 fusion.96
  127.9 0.3 copy-done.1
  128.3 2.1 fusion.98
  130.4 3.6 multiply_reduce_fusion.4
  134.1 3.0 fusion.96
  137.1 0.3 copy-done.1
  137.5 2.1 fusion.98
  139.7 3.6 multiply_reduce_fusion.4
  143.3 3.0 fusion.96
  146.4 0.3 copy-done.1
  146.7 2.1 fusion.98
  148.9 3.6 multiply_reduce_fusion.4
  152.5 3.0 fusion.96
  155.6 0.3 copy-done.1
  155.9 2.1 fusion.98
  158.1 3.6 multiply_reduce_fusion.4
  161.7 3.0 fusion.96
  164.8 0.3 copy-done.1
  165.2 2.1 fusion.98
  167.3 0.3 divide_convert_fusion
  167.7 0.4 copy.51
  168.1 1.0 all_to_all.20
  169.1 3.7 all-to-all-start
  173.2 8.1 %all-to-all-done = bf16[4,128,512]{2,1,0:T(8,128)(2,1)S(1)} async-done(((bf16[4,128,512]{2,1,0:T(8,128)(2,1)}), bf16[4,128,512]{2,1,0:T(8,128)(2,1)S(1)}, u32[]{:S(2)}, u32[]{:S(2)}) %all-to-all-start) | async-done | bytes 524320 | tf_op jit(solution)/shard_map/all_to_all | solution.py:122
  181.6 4.7 %multiply_reduce_fusion.1 = (f32[128]{0:T(128)S(1)}, f32[128,2048]{1,0:T(8,128)S(1)}) fusion(bf16[128,2048]{0,1:T(8,128)(2,1)S(1)} %bitcast.106, bf16[2048,2048]{1,0:T(8,128)(2,1)} %param.22, bf16[128,2048]{1,0:T(8,128)(2,1)S(1)} %copy-done.5), kind=kOutput, calls=%fused_computation.52 | convolution fusion | flops 1075314560 | bytes 10486272 | tf_op jit(solution)/shard_map/dot_general | solution.py:123
  186.4 1.3 convolution_convert_fusion.1
  187.8 95.8 %all_to_all.29 = bf16[32,32,2048]{2,1,0:T(8,128)(2,1)S(1)} all-to-all(bf16[32,32,2048]{2,1,0:T(8,128)(2,1)S(1)} %bitcast.103), channel_id=1, replica_groups=mesh['sp'=8,'tp'=4] {'sp','tp'}, dimensions={0} | all-to-all | bytes 8388608 | tf_op jit(solution)/shard_map/all_to_all | solution.py:157
  283.6 2.0 copy-done.2
  285.6 2.3 convolution_bitcast_fusion.2
  287.9 9.1 %convolution_convert_fusion = bf16[32,32,2048]{2,1,0:T(8,128)(2,1)} fusion(bf16[32,32,2048]{2,1,0:T(8,128)(2,1)} %copy-done.2, bf16[1,256,2048]{2,1,0:T(8,128)(2,1)S(1)} %copy-done, bf16[1,2048,256]{2,1,0:T(8,128)(2,1)} %param.29, f32[32,1,32,256]{3,2,0,1:T(8,128)} %convolution_bitcast_fusion.2), kind=kOutput, calls=%fused_computation.23 | convolution fusion | flops 2151153664 | bytes 11534336 | tf_op jit(solution)/shard_map/secf,efh->sech/dot_general | solution.py:55
  297.0 4.0 all-to-all-start.2
  301.3 0.4 fusion.75
  301.7 93.0 %all-to-all-done.2 = bf16[32,32,2048]{2,1,0:T(8,128)(2,1)} async-done(((bf16[32,32,2048]{2,1,0:T(8,128)(2,1)}), bf16[32,32,2048]{2,1,0:T(8,128)(2,1)}, u32[]{:S(2)}, u32[]{:S(2)}) %all-to-all-start.2) | async-done | bytes 4194336 | tf_op jit(solution)/shard_map/all_to_all | solution.py:162
  394.7 8.0 %gather_fusion = bf16[512,2048]{1,0:T(8,128)(2,1)} fusion(bf16[1024,2048]{1,0:T(8,128)(2,1)} %bitcast.29, s32[1024]{0:T(1024)S(1)} %pad_clamp_fusion), kind=kCustom, calls=%fused_computation | custom fusion | bytes 4196352 | tf_op jit(solution)/shard_map/gather | solution.py:165
  402.7 4.2 reshape.478
  406.9 3.8 fusion.76
  410.7 3.3 fusion.19
  (77 shorter events, 2.2 us)
Async XLA Ops:
  6.5 281.3 %copy-start = (bf16[1,256,2048]{2,1,0:T(8,128)(2,1)S(1)}, bf16[1,256,2048]{2,1,0:T(8,128)(2,1)}, u32[]{:S(2)}) copy-start(bf16[1,256,2048]{2,1,0:T(8,128)(2,1)} %param.30) | copy-start | bytes 3145732
  6.5 7.9 %copy-start.9 = (f32[128]{0:T(128)S(1)}, f32[128]{0:T(128)}, u32[]{:S(2)}) copy-start(f32[128]{0:T(128)} %param.23) | copy-start | bytes 1540
  6.5 45.6 %all-gather.6.cloned.1.call-start = ((), (), s32[]{:S(2)}) async-start(), calls=%async_computation.4 | async-start | bytes 1179648 | tf_op jit(solution)/shard_map/all_gather | solution.py:92
  9.7 83.8 %all-gather.4.cloned.1.call-start = ((), (), s32[]{:S(2)}) async-start(), calls=%async_computation.3 | async-start | bytes 1179648 | tf_op jit(solution)/shard_map/all_gather | solution.py:93
  15.2 3.5 copy-start.7
  97.2 3.4 copy-start.1
  106.4 3.4 copy-start.1
  115.6 3.4 copy-start.1
  124.8 3.4 copy-start.1
  134.0 3.4 copy-start.1
  143.3 3.4 copy-start.1
  152.5 3.4 copy-start.1
  161.7 3.4 copy-start.1
  167.3 14.3 %copy-start.5 = (bf16[128,2048]{1,0:T(8,128)(2,1)S(1)}, bf16[128,2048]{1,0:T(8,128)(2,1)}, u32[]{:S(2)}) copy-start(bf16[128,2048]{1,0:T(8,128)(2,1)} %param.21) | copy-start | bytes 1572868
  169.1 12.3 %all-to-all-start = ((bf16[4,128,512]{2,1,0:T(8,128)(2,1)}), bf16[4,128,512]{2,1,0:T(8,128)(2,1)S(1)}, u32[]{:S(2)}, u32[]{:S(2)}) async-start(bf16[4,128,512]{2,1,0:T(8,128)(2,1)} %all_to_all.20), calls=%async_computation | async-start | bytes 1048576 | tf_op jit(solution)/shard_map/all_to_all | solution.py:122
  181.6 4.8 %copy-start.6 = (f32[2048]{0:T(1024)S(1)}, f32[2048]{0:T(1024)}, u32[]{:S(2)}) copy-start(f32[2048]{0:T(1024)} %param.25) | copy-start | bytes 24580
  187.7 97.8 %copy-start.10 = (bf16[1,2048,256]{2,1,0:T(8,128)(2,1)S(1)}, bf16[1,2048,256]{2,1,0:T(8,128)(2,1)}, u32[]{:S(2)}) copy-start(bf16[1,2048,256]{2,1,0:T(8,128)(2,1)} %param.28) | copy-start | bytes 3145732
  283.6 2.0 copy-start.2
  297.0 4.1 copy-start.8
  297.0 4.3 %copy-start.4 = (bf16[2048,256]{1,0:T(8,128)(2,1)S(1)}, bf16[2048,256]{1,0:T(8,128)(2,1)}, u32[]{:S(2)}) copy-start(bf16[2048,256]{1,0:T(8,128)(2,1)} %param.31) | copy-start | bytes 3145732
  297.0 97.7 %all-to-all-start.2 = ((bf16[32,32,2048]{2,1,0:T(8,128)(2,1)}), bf16[32,32,2048]{2,1,0:T(8,128)(2,1)}, u32[]{:S(2)}, u32[]{:S(2)}) async-start(bf16[32,32,2048]{2,1,0:T(8,128)(2,1)} %convolution_convert_fusion), calls=%async_computation.2 | async-start | bytes 8388608 | tf_op jit(solution)/shard_map/all_to_all | solution.py:162
  402.7 8.0 %copy-start.3 = (bf16[256,2048]{1,0:T(8,128)(2,1)S(1)}, bf16[256,2048]{1,0:T(8,128)(2,1)}, u32[]{:S(2)}) copy-start(bf16[256,2048]{1,0:T(8,128)(2,1)} %param.33) | copy-start | bytes 3145732
Sparse Core Ops, SparseCore 0:
  9.9 42.2 all-gather.5
  54.2 39.2 all-gather.3
where the time goes:
time: 422 us; the launch traced here: 421 us
  waiting for transfers between devices  176 us (42%)
  blocking collectives  95.8 us (23%)
  matrix products  71 us (17%)
  other arithmetic  34.1 us (8%)
  local copies, waits for them, and re-layouts  21.8 us (5%)
  between operations  13.7 us (3%)
  starting transfers between devices  7.71 us (2%)
    all_to_all x1, blocking collectives, body(): lax.all_to_all(send_rows, ('sp', 'tp'), split_axis=0, concat_axis=0, tile...  95.8 us
    all_to_all x1, waiting for transfers between devices, body(): lax.all_to_all(processed, ('sp', 'tp'), split_axis=0, concat_axis=0, tile...  93 us
    all_gather x1, waiting for transfers between devices, body(): value_piece = lax.all_gather(values, 'sp', axis=0, tiled=True)  41.4 us
    all_gather x1, waiting for transfers between devices, body(): key_piece = lax.all_gather(k_rot, 'sp', axis=0, tiled=True)  32.9 us
    dot_general x8, matrix products, one_block(): jnp.einsum('gqd,kgd->gqk', query_3d, key_3d, preferred_element_type=jnp.f...  28.8 us
    reduce_sum x8, other arithmetic, one_block(): new_sum = running_sum * factor + jnp.sum(weights, axis=-1)  24.4 us
    dot_general x8, matrix products, one_block(): jnp.einsum('gqk,kgd->gqd', weights.astype(jnp.bfloat16), value_3d, prefer...  17.1 us
    dot_general x1, matrix products, expert_apply(): jnp.einsum('secf,efh->sech', hidden_e, expert_down, preferred_element_typ...  9.08 us
  transfers between devices with their start and end apart: 4, of which 4 were waited for; matrix products, arithmetic and copies ran while one was open for 2% of the time, Pallas kernels for 0%

commit v1 on v0

--- a/solution.py
+++ b/solution.py
@@ -89,8 +89,11 @@
         jnp.zeros((kv_local, group * tok_local), jnp.float32),
         jnp.zeros((kv_local, group * tok_local, width), jnp.float32),
     )
-    key_piece = lax.all_gather(k_rot, "sp", axis=0, tiled=True)
-    value_piece = lax.all_gather(values, "sp", axis=0, tiled=True)
+    key_piece, value_piece = jnp.split(
+        lax.all_gather(jnp.concatenate([k_rot, values], 1), "sp", axis=0, tiled=True),
+        [k_rot.shape[1]],
+        1,
+    )
     count = key_piece.shape[0]
     block = math.gcd(count, 512)
 

time: 422 us -> 394 us (0.934)
  waiting for transfers between devices: 176 us -> 146 us
    all_gather x2 -> x1, waiting for transfers between devices: 74.4 us -> 44.5 us  [body(): lax.all_gather(jnp.concatenate([k_rot, values], 1), 'sp', axis=0, tiled=T...]
  transfers between devices with their start and end apart: 4 -> 3, of which waited for: 4 -> 3; matrix products, arithmetic and copies ran while one was open for 2% -> 2% of each run, Pallas kernels for 0% -> 0%
where the time goes in v1:
time: 394 us
  waiting for transfers between devices  146 us (37%)
  blocking collectives  95.5 us (24%)
  matrix products  70.7 us (18%)
  other arithmetic  34.2 us (9%)
  local copies, waits for them, and re-layouts  25.9 us (7%)
  between operations  13.7 us (3%)
  starting transfers between devices  7.6 us (2%)
    all_to_all x1, blocking collectives, body(): lax.all_to_all(send_rows, ('sp', 'tp'), split_axis=0, concat_axis=0, tile...  95.5 us
    all_to_all x1, waiting for transfers between devices, body(): lax.all_to_all(processed, ('sp', 'tp'), split_axis=0, concat_axis=0, tile...  93 us
    all_gather x1, waiting for transfers between devices, body(): lax.all_gather(jnp.concatenate([k_rot, values], 1), 'sp', axis=0, tiled=T...  44.5 us
    dot_general x8, matrix products, one_block(): jnp.einsum('gqd,kgd->gqk', query_3d, key_3d, preferred_element_type=jnp.f...  28.6 us
    reduce_sum x8, other arithmetic, one_block(): new_sum = running_sum * factor + jnp.sum(weights, axis=-1)  24.4 us
    dot_general x8, matrix products, one_block(): jnp.einsum('gqk,kgd->gqd', weights.astype(jnp.bfloat16), value_3d, prefer...  16.9 us
    dot_general x1, matrix products, expert_apply(): jnp.einsum('secf,efh->sech', hidden_e, expert_down, preferred_element_typ...  9.07 us
    all_to_all x1, waiting for transfers between devices, body(): lax.all_to_all(attn_local, 'tp', split_axis=0, concat_axis=1, tiled=True)  8.13 us
  transfers between devices with their start and end apart: 3, of which 3 were waited for; matrix products, arithmetic and copies ran while one was open for 2% of the time, Pallas kernels for 0%

profile of v1, /device:TPU:0, one launch (start us, length us, event | category | flops | bytes accessed | tf_op | source)
XLA Modules:
  0.0 393.6 jit_solution(12683018205768213622)
XLA Ops:
  6.6 1.1 copy.36
  7.7 1.0 copy.35
  8.8 0.7 fusion.43
  9.5 0.6 fusion.62
  10.1 0.7 pad_maximum_fusion
  10.9 1.4 reshape.480
  12.2 0.6 multiply_reduce_fusion.2
  12.9 1.9 multiply_cosine_fusion.1
  14.8 0.7 multiply_multiply_fusion
  15.5 1.8 fusion.37
  17.3 1.6 maximum_bitcast_fusion
  19.5 44.5 %all-gather.2.cloned.1.call-done = bf16[4096,256]{0,1:T(8,128)(2,1)} async-done(((bf16[512,256]{0,1:T(8,128)(2,1)}), bf16[4096,256]{0,1:T(8,128)(2,1)}) %all-gather.2.cloned.1.call-update) | async-done | bytes 2097168 | tf_op jit(solution)/shard_map/all_gather | solution.py:93
  64.1 3.1 fusion.76
  67.1 73.4 %while.18 = (s32[]{:T(128)}, f32[1,2048]{1,0:T(1,128)S(1)}, f32[1,2048]{1,0:T(1,128)S(1)}, f32[1,2048,128]{2,1,0:T(8,128)S(1)}, bf16[4096,128]{0,1:T(8,128)(2,1)...) while((s32[]{:T(128)}, f32[1,2048]{1,0:T(1,128)S(1)}, ...), condition=%wide.region_5.6_spmd.clone, body=%wide.region_2.5_spmd.clone.sunk | while | flops 546056192 | bytes 32374992 | solution.py:121
  67.1 3.6 multiply_reduce_fusion.4
  70.7 3.0 fusion.97
  73.8 0.3 copy-done.1
  74.2 2.1 fusion.99
  76.3 3.6 multiply_reduce_fusion.4
  79.9 3.0 fusion.97
  83.0 0.3 copy-done.1
  83.3 2.1 fusion.99
  85.5 3.6 multiply_reduce_fusion.4
  89.1 3.0 fusion.97
  92.2 0.3 copy-done.1
  92.5 2.1 fusion.99
  94.7 3.6 multiply_reduce_fusion.4
  98.3 3.0 fusion.97
  101.4 0.3 copy-done.1
  101.7 2.1 fusion.99
  103.8 3.6 multiply_reduce_fusion.4
  107.4 3.0 fusion.97
  110.5 0.3 copy-done.1
  110.9 2.1 fusion.99
  113.0 3.6 multiply_reduce_fusion.4
  116.6 3.0 fusion.97
  119.7 0.3 copy-done.1
  120.0 2.1 fusion.99
  122.2 3.6 multiply_reduce_fusion.4
  125.8 3.0 fusion.97
  128.9 0.3 copy-done.1
  129.2 2.1 fusion.99
  131.4 3.6 multiply_reduce_fusion.4
  135.0 3.0 fusion.97
  138.1 0.3 copy-done.1
  138.4 2.1 fusion.99
  140.5 0.3 divide_convert_fusion
  140.9 0.4 copy.54
  141.3 1.0 all_to_all.20
  142.3 3.7 all-to-all-start
  146.4 8.1 %all-to-all-done = bf16[4,128,512]{2,1,0:T(8,128)(2,1)S(1)} async-done(((bf16[4,128,512]{2,1,0:T(8,128)(2,1)}), bf16[4,128,512]{2,1,0:T(8,128)(2,1)S(1)}, u32[]{:S(2)}, u32[]{:S(2)}) %all-to-all-start) | async-done | bytes 524320 | tf_op jit(solution)/shard_map/all_to_all | solution.py:125
  154.9 4.7 %multiply_reduce_fusion.1 = (f32[128]{0:T(128)S(1)}, f32[128,2048]{1,0:T(8,128)S(1)}) fusion(bf16[128,2048]{0,1:T(8,128)(2,1)S(1)} %bitcast.107, bf16[2048,2048]{1,0:T(8,128)(2,1)} %param.22, bf16[128,2048]{1,0:T(8,128)(2,1)S(1)} %copy-done.5), kind=kOutput, calls=%fused_computation.52 | convolution fusion | flops 1075314560 | bytes 10486272 | tf_op jit(solution)/shard_map/dot_general | solution.py:126
  159.6 1.3 convolution_convert_fusion.1
  161.0 95.5 %all_to_all.29 = bf16[32,32,2048]{2,1,0:T(8,128)(2,1)S(1)} all-to-all(bf16[32,32,2048]{2,1,0:T(8,128)(2,1)S(1)} %bitcast.104), channel_id=1, replica_groups=mesh['sp'=8,'tp'=4] {'sp','tp'}, dimensions={0} | all-to-all | bytes 8388608 | tf_op jit(solution)/shard_map/all_to_all | solution.py:160
  256.5 2.0 copy-done.2
  258.4 2.3 convolution_bitcast_fusion.2
  260.8 9.1 %convolution_convert_fusion = bf16[32,32,2048]{2,1,0:T(8,128)(2,1)} fusion(bf16[32,32,2048]{2,1,0:T(8,128)(2,1)} %copy-done.2, bf16[1,256,2048]{2,1,0:T(8,128)(2,1)S(1)} %copy-done, bf16[1,2048,256]{2,1,0:T(8,128)(2,1)} %param.29, f32[32,1,32,256]{3,2,0,1:T(8,128)} %convolution_bitcast_fusion.2), kind=kOutput, calls=%fused_computation.23 | convolution fusion | flops 2151153664 | bytes 11534336 | tf_op jit(solution)/shard_map/secf,efh->sech/dot_general | solution.py:55
  269.8 3.9 %all-to-all-start.2 = ((bf16[32,32,2048]{2,1,0:T(8,128)(2,1)}), bf16[32,32,2048]{2,1,0:T(8,128)(2,1)}, u32[]{:S(2)}, u32[]{:S(2)}) async-start(bf16[32,32,2048]{2,1,0:T(8,128)(2,1)} %convolution_convert_fusion), calls=%async_computation.2 | async-start | bytes 8388608 | tf_op jit(solution)/shard_map/all_to_all | solution.py:165
  274.1 0.4 fusion.75
  274.5 93.0 %all-to-all-done.2 = bf16[32,32,2048]{2,1,0:T(8,128)(2,1)} async-done(((bf16[32,32,2048]{2,1,0:T(8,128)(2,1)}), bf16[32,32,2048]{2,1,0:T(8,128)(2,1)}, u32[]{:S(2)}, u32[]{:S(2)}) %all-to-all-start.2) | async-done | bytes 4194336 | tf_op jit(solution)/shard_map/all_to_all | solution.py:165
  367.5 8.0 %gather_fusion = bf16[512,2048]{1,0:T(8,128)(2,1)} fusion(bf16[1024,2048]{1,0:T(8,128)(2,1)} %bitcast.29, s32[1024]{0:T(1024)S(1)} %pad_clamp_fusion), kind=kCustom, calls=%fused_computation | custom fusion | bytes 4196352 | tf_op jit(solution)/shard_map/gather | solution.py:168
  375.5 4.2 %reshape.478 = bf16[128,4,2048]{2,1,0:T(4,128)(2,1)} reshape(bf16[512,2048]{1,0:T(8,128)(2,1)} %gather_fusion) | data formatting | bytes 4194304 | tf_op jit(solution)/shard_map/reshape | solution.py:168
  379.7 3.8 fusion.77
  383.5 3.3 fusion.19
  (77 shorter events, 2.2 us)
Async XLA Ops:
  6.5 254.2 %copy-start = (bf16[1,256,2048]{2,1,0:T(8,128)(2,1)S(1)}, bf16[1,256,2048]{2,1,0:T(8,128)(2,1)}, u32[]{:S(2)}) copy-start(bf16[1,256,2048]{2,1,0:T(8,128)(2,1)} %param.30) | copy-start | bytes 3145732
  6.5 8.3 %copy-start.9 = (f32[128]{0:T(128)S(1)}, f32[128]{0:T(128)}, u32[]{:S(2)}) copy-start(f32[128]{0:T(128)} %param.23) | copy-start | bytes 1540
  6.5 57.5 %all-gather.2.cloned.1.call-start = ((), (), s32[]{:S(2)}) async-start(), calls=%async_computation.3 | async-start | bytes 2359296 | tf_op jit(solution)/shard_map/all_gather | solution.py:93
  15.5 3.5 copy-start.7
  70.7 3.4 copy-start.1
  79.9 3.4 copy-start.1
  89.1 3.4 copy-start.1
  98.2 3.4 copy-start.1
  107.4 3.4 copy-start.1
  116.6 3.4 copy-start.1
  125.8 3.4 copy-start.1
  134.9 3.4 copy-start.1
  140.5 14.3 %copy-start.5 = (bf16[128,2048]{1,0:T(8,128)(2,1)S(1)}, bf16[128,2048]{1,0:T(8,128)(2,1)}, u32[]{:S(2)}) copy-start(bf16[128,2048]{1,0:T(8,128)(2,1)} %param.21) | copy-start | bytes 1572868
  142.3 12.3 %all-to-all-start = ((bf16[4,128,512]{2,1,0:T(8,128)(2,1)}), bf16[4,128,512]{2,1,0:T(8,128)(2,1)S(1)}, u32[]{:S(2)}, u32[]{:S(2)}) async-start(bf16[4,128,512]{2,1,0:T(8,128)(2,1)} %all_to_all.20), calls=%async_computation | async-start | bytes 1048576 | tf_op jit(solution)/shard_map/all_to_all | solution.py:125
  154.8 4.8 %copy-start.6 = (f32[2048]{0:T(1024)S(1)}, f32[2048]{0:T(1024)}, u32[]{:S(2)}) copy-start(f32[2048]{0:T(1024)} %param.25) | copy-start | bytes 24580
  161.0 97.5 %copy-start.10 = (bf16[1,2048,256]{2,1,0:T(8,128)(2,1)S(1)}, bf16[1,2048,256]{2,1,0:T(8,128)(2,1)}, u32[]{:S(2)}) copy-start(bf16[1,2048,256]{2,1,0:T(8,128)(2,1)} %param.28) | copy-start | bytes 3145732
  256.5 2.0 copy-start.2
  269.8 4.1 %copy-start.8 = (f32[128,4]{0,1:T(4,128)S(1)}, f32[128,4]{0,1:T(4,128)}, u32[]{:S(2)}) copy-start(f32[128,4]{0,1:T(4,128)} %param.27) | copy-start | bytes 6148
  269.8 4.3 %copy-start.4 = (bf16[2048,256]{1,0:T(8,128)(2,1)S(1)}, bf16[2048,256]{1,0:T(8,128)(2,1)}, u32[]{:S(2)}) copy-start(bf16[2048,256]{1,0:T(8,128)(2,1)} %param.31) | copy-start | bytes 3145732
  269.8 97.6 %all-to-all-start.2 = ((bf16[32,32,2048]{2,1,0:T(8,128)(2,1)}), bf16[32,32,2048]{2,1,0:T(8,128)(2,1)}, u32[]{:S(2)}, u32[]{:S(2)}) async-start(bf16[32,32,2048]{2,1,0:T(8,128)(2,1)} %convolution_convert_fusion), calls=%async_computation.2 | async-start | bytes 8388608 | tf_op jit(solution)/shard_map/all_to_all | solution.py:165
  375.5 8.0 %copy-start.3 = (bf16[256,2048]{1,0:T(8,128)(2,1)S(1)}, bf16[256,2048]{1,0:T(8,128)(2,1)}, u32[]{:S(2)}) copy-start(bf16[256,2048]{1,0:T(8,128)(2,1)} %param.33) | copy-start | bytes 3145732
Sparse Core Ops, SparseCore 0:
  11.0 53.0 all-gather.1
